TPU v7x, 32 devices: a whole 2x2x4 slice. The times are simulated.
32 devices in a mesh: fs: 8 (over z, x), tp: 4 (over y, core).
Axes of the slice: x: 2, y: 2, z: 4, core: 2. Of those that a mesh axis runs over, the one named last changes fastest.
Arguments:
- seq_rows: bfloat16 [6144, 2048], P('fs', 'tp'), may hold values from -6 to 6
- mixer_gain: bfloat16 [2048], P('tp'), may hold values from 0.099609375 to 1.8984375
- query_weight: bfloat16 [2048, 2048], P('fs', 'tp'), may hold values from -0.125 to 0.125
- key_weight: bfloat16 [2048, 2048], P('fs', 'tp'), may hold values from -0.125 to 0.125
- value_weight: bfloat16 [2048, 4096], P('fs', 'tp'), may hold values from -0.125 to 0.125
- decay_logs: float32 [8], P('tp'), may hold values from -0.0333333333 to -0.000390625
- mixer_out_weight: bfloat16 [4096, 2048], P('tp', 'fs'), may hold values from -0.125 to 0.125
- channel_gain: bfloat16 [2048], P('tp'), may hold values from 0.099609375 to 1.8984375
- value_up_weight: bfloat16 [2048, 5632], P('fs', 'tp'), may hold values from -0.125 to 0.125
- gate_up_weight: bfloat16 [2048, 5632], P('fs', 'tp'), may hold values from -0.125 to 0.125
- conv_taps: bfloat16 [3, 5632], P(None, 'tp'), may hold values from -3 to 3
- conv_bias: bfloat16 [5632], P('tp'), may hold values from -3 to 3
- down_weight: bfloat16 [5632, 2048], P('tp', 'fs'), may hold values from -0.109375 to 0.109375
Outputs:
- layer_out: bfloat16 [6144, 2048], P('fs', 'tp')
All inputs are finite; a program needn't handle non-finite values.
Results may differ from a plain program's by a relative error of at most 0.02.
Values may be sent and summed in bfloat16 or wider, within the bound.
A program may use at most 128 MiB of HBM per device.

v0:
```python
import functools

import jax
import jax.numpy as jnp
import numpy as np
from jax import lax
from jax.experimental import pallas as pl
from jax.experimental.pallas import tpu as pltpu
from jax.sharding import PartitionSpec as P

DK = 256
DV = 512
KW = 3
EPS = 1e-06
ROPE_BASE = 10000.0
LANES = 128
ROWS = 256
PAD = 8
BF16 = jnp.bfloat16
F32 = jnp.float32


def flip(index, mask):
    return index + mask * (1 - 2 * lax.rem(lax.div(index, mask), 2))


def flips(index, mask):
    bit = 1
    while bit <= mask:
        if mask & bit:
            index = flip(index, bit)
        bit *= 2
    return index


def bits_of(size):
    return [1 << i for i in range(size.bit_length() - 1)]


class Plan:
    def __init__(self, fs, tp, length, block, heads_here, ff_here, shard):
        self.fs, self.tp, self.length, self.block, self.shard = fs, tp, length, block, shard
        self.width = fs * shard
        self.paired = heads_here % 2 == 0 and ff_here % LANES == 0 and fs >= 4
        self.heads = heads_here // 2 if self.paired else heads_here
        self.ff = -(-ff_here // (2 * LANES)) * LANES if self.paired else ff_here
        self.ff_step = ff_here - self.ff
        self.seqs = 2 if self.paired else 1
        self.rows = self.seqs * length
        self.pair = 2 if self.paired else 0
        self.gather = ([self.pair] if self.paired else []) + [b for b in bits_of(fs)[::-1] if b != self.pair]
        self.dims = [("tp", b) for b in bits_of(tp)] + ([("fs", self.pair)] if self.paired else [])
        self.qk = self.heads * DK
        self.dv = self.heads * DV
        self.heads_step = self.heads


class Mail:
    def __init__(self, sends, recvs, me):
        self.sends, self.recvs, self.me = sends, recvs, me
        self.count = 0
        self.ids = {}
        self.sent = []

    def id_of(self, key):
        if key not in self.ids:
            self.ids[key] = len(self.ids)
        return self.ids[key]

    def copy(self, key, src, dst, axis, mask):
        n = self.id_of(key)
        return pltpu.make_async_remote_copy(
            src_ref=src,
            dst_ref=dst,
            send_sem=self.sends.at[n],
            recv_sem=self.recvs.at[n],
            device_id={axis: flip(self.me[axis], mask)},
            device_id_type=pl.DeviceIdType.MESH,
        )

    def send(self, key, src, dst, axis, mask):
        copy = self.copy(key, src, dst, axis, mask)
        copy.start()
        self.sent.append(copy)
        return copy

    def arrive(self, key, slot, axis, mask):
        self.copy(key, slot, slot, axis, mask).wait_recv()

    def drain(self):
        for copy in self.sent:
            copy.wait_send()
        self.sent = []


class Stream:
    def __init__(self, plan, mail, name, slot, stage):
        self.plan, self.mail, self.name, self.slot, self.stage = plan, mail, name, slot, stage
        self.mine = mail.me["fs"]
        self.bits = plan.gather

    def at(self, code):
        return self.slot(flips(self.mine, code))

    def forward(self, code, first):
        for bit in self.bits[first:]:
            src = self.stage if bit == self.plan.pair else self.at(code)
            self.mail.send((self.name, bit, code), src, self.at(code), "fs", bit)

    def begin(self):
        self.forward(0, 0)
        self.todo = []
        codes = [0]
        for place, bit in enumerate(self.bits):
            new = [c | bit for c in codes]
            self.todo += [(c, bit, place) for c in new]
            codes = codes + new

    def step(self, times=1):
        for _ in range(times):
            if self.todo:
                code, bit, place = self.todo.pop(0)
                self.mail.arrive((self.name, bit, code & ~bit), self.at(code), "fs", bit)
                self.forward(code, place + 1)

    def steps_left(self):
        return sum(1 for t in self.todo if t[2] < len(self.bits) - 1)

    def finish(self):
        self.step(len(self.todo))


def kernel(
    plan,
    x_hbm, gain_hbm, cos_hbm, sin_hbm, q_hbm, k_hbm, v_hbm, decay, out_hbm, val_hbm, gate_hbm, conv_hbm, down_hbm,
    result,
    w_in, w_out, w_val, w_gate, w_down, s_in, s_out, s_val, s_gate, s_down,
    act, act2, gains, cosine, sine, conv_par, qk, value, normed, part, hidden, gates,
    *rest,
):
    n_dims = len(plan.dims)
    recvs, outs = rest[:n_dims], rest[n_dims : 2 * n_dims - 1]
    sends, arrivals, local = rest[2 * n_dims - 1 :]
    me = {"fs": lax.axis_index("fs"), "tp": lax.axis_index("tp")}
    length, block, shard = plan.length, plan.block, plan.shard
    row_blocks = length // ROWS
    seq = lax.rem(lax.div(me["fs"], plan.pair), 2) if plan.paired else 0

    barrier = pltpu.get_barrier_semaphore()
    near = [("fs", b) for b in plan.gather] + [d for d in plan.dims if d[0] == "tp"]
    for axis, bit in near:
        pl.semaphore_signal(
            barrier, inc=1, device_id={axis: flip(me[axis], bit)}, device_id_type=pl.DeviceIdType.MESH
        )

    places = []

    def fetch(src, dst):
        copy = pltpu.make_async_copy(src, dst, local.at[len(places)])
        copy.start()
        places.append(copy)

    def columns(index, width, size=None):
        return pl.ds(pl.multiple_of(index * width, width), size or width)

    def own_block(ref, s, t):
        return ref.at[columns(s, length), columns(t, block)]

    fetch(x_hbm, own_block(act, seq, me["tp"]))
    fetch(gain_hbm, gains.at[:, columns(me["tp"], block)])
    mine = me["fs"]
    rows_in = columns(mine, shard)

    def halves(dst, stage, take):
        fetch(take(seq), dst)
        if plan.paired:
            fetch(take(1 - seq), stage)

    qk_w, dv_w = plan.qk, plan.dv
    halves(w_in.at[rows_in, 0:qk_w], s_in.at[:, 0:qk_w], lambda h: q_hbm.at[:, columns(h, qk_w)])
    halves(
        w_in.at[rows_in, qk_w : 2 * qk_w], s_in.at[:, qk_w : 2 * qk_w], lambda h: k_hbm.at[:, columns(h, qk_w)]
    )
    halves(
        w_in.at[rows_in, 2 * qk_w : 2 * qk_w + dv_w],
        s_in.at[:, 2 * qk_w : 2 * qk_w + dv_w],
        lambda h: v_hbm.at[:, columns(h, dv_w)],
    )
    n_first = len(places)
    halves(w_out.at[:, columns(mine, shard)], s_out, lambda h: out_hbm.at[columns(h, dv_w), :])

    def ff_part(h):
        if not plan.paired:
            return slice(None)
        return pl.ds(pl.multiple_of(h * plan.ff_step, LANES), plan.ff)

    halves(w_val.at[rows_in, :], s_val, lambda h: val_hbm.at[:, ff_part(h)])
    halves(w_gate.at[rows_in, :], s_gate, lambda h: gate_hbm.at[:, ff_part(h)])
    halves(w_down.at[:, columns(mine, shard)], s_down, lambda h: down_hbm.at[ff_part(h), :])
    fetch(cos_hbm, cosine)
    fetch(sin_hbm, sine)
    fetch(conv_hbm.at[:, ff_part(seq)], conv_par)

    mail = Mail(sends, arrivals, me)
    st_in = Stream(plan, mail, "in", lambda j: w_in.at[columns(j, shard), :], s_in)
    st_out = Stream(plan, mail, "out", lambda j: w_out.at[:, columns(j, shard)], s_out)
    st_val = Stream(plan, mail, "val", lambda j: w_val.at[columns(j, shard), :], s_val)
    st_gate = Stream(plan, mail, "gate", lambda j: w_gate.at[columns(j, shard), :], s_gate)
    st_down = Stream(plan, mail, "down", lambda j: w_down.at[:, columns(j, shard)], s_down)

    def seq_of(code):
        return 1 - seq if plan.paired and code >> (n_dims - 1) else seq

    def tp_of(code):
        return flips(me["tp"], code & (plan.tp - 1))

    class Gather:
        def __init__(self, name, at, dims):
            self.name, self.at, self.dims = name, at, dims
            self.todo = []

        def forward(self, code, last):
            for place in range(last - 1, -1, -1):
                axis, bit = self.dims[place]
                mail.send((self.name, place, code), self.at(code), self.at(code), axis, bit)

        def begin(self):
            self.forward(0, len(self.dims))
            codes = [0]
            for place in range(len(self.dims) - 1, -1, -1):
                new = [c | (1 << place) for c in codes]
                self.todo += [(c, place) for c in new]
                codes = codes + new

        def step(self, times):
            for _ in range(times):
                code, place = self.todo.pop(0)
                axis, bit = self.dims[place]
                mail.arrive((self.name, place, code & ~(1 << place)), self.at(code), axis, bit)
                self.forward(code, place)

        def finish(self):
            self.step(len(self.todo))

    tp_dims = [d for d in plan.dims if d[0] == "tp"]
    gather_gain = Gather("gain", lambda c: gains.at[:, columns(tp_of(c), block)], tp_dims)
    gather_one = Gather("one", lambda c: own_block(act, seq_of(c), tp_of(c)), plan.dims)
    gather_two = Gather("two", lambda c: own_block(act2, seq_of(c), tp_of(c)), plan.dims)

    for copy in places[:n_first]:
        copy.wait()
    pl.semaphore_wait(barrier, len(near))
    gather_one.begin()
    gather_gain.begin()
    st_in.begin()
    for copy in places[n_first:]:
        copy.wait()
    gather_one.step(1)
    st_in.step(1)
    st_out.begin()
    gather_one.step(2)
    gather_gain.step(1)
    st_in.step(1)
    st_val.begin()
    st_in.step(1)
    st_out.step(1)
    gather_one.finish()
    gather_gain.finish()
    st_out.step(1)
    st_gate.begin()
    st_in.finish()

    def scaled_rows(ref, start, gain_row):
        rows_f = ref[pl.ds(start, ROWS), :].astype(F32)
        factor = lax.rsqrt(jnp.mean(rows_f * rows_f, axis=-1, keepdims=True) + EPS)
        gain = gains[gain_row : gain_row + 1, :].astype(F32)
        return (rows_f * gain).astype(BF16), factor

    def project(i, _):
        start = pl.multiple_of(i * ROWS, ROWS)
        spot = pl.ds(pl.multiple_of(lax.rem(i, row_blocks) * ROWS, ROWS), ROWS)
        scaled, factor = scaled_rows(act, start, 0)
        total = jnp.dot(scaled, w_in[...], preferred_element_type=F32)
        cos, sin = cosine[spot, :], sine[spot, :]
        half = DK // 2
        for which, scale in ((0, 1.0), (1, DK**-0.5)):
            for head in range(plan.heads):
                at = which * qk_w + head * DK
                turned = (total[:, at : at + DK] * factor).astype(BF16).astype(F32)
                one, two = turned[:, :half], turned[:, half:]
                qk[pl.ds(start, ROWS), at : at + half] = ((one * cos - two * sin) * scale).astype(BF16)
                qk[pl.ds(start, ROWS), at + half : at + DK] = ((one * sin + two * cos) * scale).astype(BF16)
        value[pl.ds(start, ROWS), :] = (total[:, 2 * qk_w :] * factor).astype(BF16)
        return 0

    lax.fori_loop(0, plan.rows // ROWS, project, 0)
    st_out.step(1)
    st_val.step(1)

    def retain(s, _):
        for head in range(plan.heads):
            log_decay = decay[seq * plan.heads + head]
            for b in range(row_blocks):
                seen = (b + 1) * ROWS
                first = pl.multiple_of(s * length, ROWS)
                rows = pl.ds(pl.multiple_of(first + b * ROWS, ROWS), ROWS)
                keys = pl.ds(first, seen)
                query = qk[rows, head * DK : (head + 1) * DK]
                key = qk[keys, qk_w + head * DK : qk_w + (head + 1) * DK]
                scores = lax.dot_general(query, key, (((1,), (1,)), ((), ())), preferred_element_type=F32)
                spread = (
                    lax.broadcasted_iota(jnp.int32, (ROWS, seen), 0)
                    - lax.broadcasted_iota(jnp.int32, (ROWS, seen), 1)
                    + b * ROWS
                )
                fall = jnp.exp(log_decay * jnp.maximum(spread, 0).astype(F32))
                scores = jnp.where(spread >= 0, scores * fall, 0.0).astype(BF16)
                ret = jnp.dot(scores, value[keys, head * DV : (head + 1) * DV], preferred_element_type=F32)
                centred = ret - jnp.mean(ret, axis=-1, keepdims=True)
                scale = lax.rsqrt(jnp.mean(centred * centred, axis=-1, keepdims=True) + EPS)
                normed[rows, head * DV : (head + 1) * DV] = (centred * scale).astype(BF16)
        return 0

    lax.fori_loop(0, plan.seqs, retain, 0)
    st_out.finish()

    n_codes = 1 << n_dims

    def block_rows(s, i):
        return pl.ds(pl.multiple_of(s * length + i * ROWS, ROWS), ROWS)

    def multiply(left, right, code):
        cols = columns(tp_of(code), block)
        s = seq_of(code)

        def body(i, _):
            rows = block_rows(s, i)
            part[rows, cols] = jnp.dot(left[rows, :], right[:, cols], preferred_element_type=F32).astype(BF16)
            return 0

        lax.fori_loop(0, row_blocks, body, 0)

    def low(code):
        return next(i for i in range(n_dims) if code >> i & 1) if code else n_dims

    def summed(code, i):
        rows = pl.ds(pl.multiple_of(i * ROWS, ROWS), ROWS)
        total = part[block_rows(seq_of(code), i), columns(tp_of(code), block)].astype(F32)
        for place in range(low(code)):
            total = total + recvs[place][code >> (place + 1), rows, :].astype(F32)
        return total

    def scatter(name, left, right, write, between):
        order = sorted(range(n_codes), key=lambda c: (low(c) > 0, -c))
        sent = []

        def ship(code, src):
            place = low(code)
            axis, bit = plan.dims[place]
            sent.append(mail.send((name, place, code), src, recvs[place].at[code >> (place + 1)], axis, bit))

        for code in order:
            multiply(left, right, code)
            if code & 1:
                ship(code, own_block(part, seq_of(code), tp_of(code)))
        for place in range(1, n_dims + 1):
            codes = [c for c in range(n_codes) if low(c) == place][::-1]
            for code in codes:
                for k in range(place):
                    axis, bit = plan.dims[k]
                    key = (name, k, code | (1 << k))
                    if key not in waited:
                        waited.add(key)
                        mail.arrive(key, recvs[k].at[code >> (k + 1)], axis, bit)
                if place < n_dims:
                    target = outs[place - 1].at[code >> (place + 1)]

                    def body(i, _):
                        rows = pl.ds(pl.multiple_of(i * ROWS, ROWS), ROWS)
                        target[rows, :] = summed(code, i).astype(BF16)
                        return 0

                    lax.fori_loop(0, row_blocks, body, 0)
                    ship(code, target)
                between()

        def body(i, _):
            write(i, summed(0, i))
            return 0

        lax.fori_loop(0, row_blocks, body, 0)
        for copy in sent:
            copy.wait_send()
        mail.sent = [c for c in mail.sent if not any(c is d for d in sent)]

    waited = set()
    queue = [st_val, st_gate]

    def pump():
        for stream in queue:
            if stream.steps_left():
                stream.step(1)
                return

    def write_middle(i, total):
        rows = pl.ds(pl.multiple_of(i * ROWS, ROWS), ROWS)
        cols = columns(me["tp"], block)
        mine_rows = block_rows(seq, i)
        act2[mine_rows, cols] = (act[mine_rows, cols].astype(F32) + total).astype(BF16)

    scatter("mixed", normed, w_out, write_middle, pump)
    gather_two.begin()
    st_down.begin()
    gather_two.step(1)
    pump()
    gather_two.step(2)
    pump()
    gather_two.finish()
    while st_gate.steps_left():
        pump()
    st_val.finish()
    st_gate.finish()
    st_down.step(1)

    gates[0:PAD, :] = jnp.zeros((PAD, plan.ff), F32)
    column = lax.broadcasted_iota(jnp.int32, (1, plan.ff), 1)
    keep = column >= seq * (plan.ff - plan.ff_step) if plan.paired else None

    def expand(i, _):
        start = pl.multiple_of(i * ROWS, ROWS)
        scaled, factor = scaled_rows(act2, start, 1)
        gate = (jnp.dot(scaled, w_gate[...], preferred_element_type=F32) * factor).astype(BF16).astype(F32)
        before = gates[ROWS : ROWS + PAD, :]
        gates[0:PAD, :] = jnp.where(lax.rem(i, row_blocks) == 0, jnp.zeros_like(before), before)
        gates[PAD : PAD + ROWS, :] = gate
        conv = conv_par[KW : KW + 1, :] + jnp.zeros((ROWS, plan.ff), F32)
        for tap in range(KW):
            at = PAD - KW + 1 + tap
            conv = conv + conv_par[tap : tap + 1, :] * gates[at : at + ROWS, :]
        up = (jnp.dot(scaled, w_val[...], preferred_element_type=F32) * factor).astype(BF16).astype(F32)
        made = conv / (1.0 + jnp.exp(-conv)) * up
        if keep is not None:
            made = jnp.where(keep, made, 0.0)
        hidden[pl.ds(start, ROWS), :] = made.astype(BF16)
        return 0

    lax.fori_loop(0, plan.rows // ROWS, expand, 0)
    st_down.finish()

    def write_result(i, total):
        rows = pl.ds(pl.multiple_of(i * ROWS, ROWS), ROWS)
        cols = columns(me["tp"], block)
        result[rows, :] = (act2[block_rows(seq, i), cols].astype(F32) + total).astype(BF16)

    scatter("channel", hidden, w_down, write_result, lambda: None)
    mail.drain()


def on_device(
    seq_rows, mixer_gain, query_weight, key_weight, value_weight, decay_logs, mixer_out_weight, channel_gain,
    value_up_weight, gate_up_weight, conv_taps, conv_bias, down_weight,
):
    length, block = seq_rows.shape
    plan = Plan(
        lax.axis_size("fs"), lax.axis_size("tp"), length, block,
        query_weight.shape[1] // DK, value_up_weight.shape[1], query_weight.shape[0],
    )
    gains = jnp.concatenate(
        [mixer_gain[None], channel_gain[None], jnp.zeros((14, block), BF16)], axis=0
    )
    conv = jnp.concatenate(
        [conv_taps, conv_bias[None], jnp.zeros((PAD - KW - 1, conv_bias.shape[0]), BF16)], axis=0
    ).astype(F32)
    freqs = np.power(np.float32(ROPE_BASE), -np.arange(DK // 2, dtype=np.float32) * np.float32(2.0) / np.float32(DK))
    angles = np.arange(length, dtype=np.float32)[:, None] * freqs[None, :].astype(np.float32)
    cosine = jnp.asarray(np.cos(angles).astype(np.float32))
    sine = jnp.asarray(np.sin(angles).astype(np.float32))
    n_dims = len(plan.dims)
    rows, ff, width, shard = plan.rows, plan.ff, plan.width, plan.shard
    made = 2 * plan.qk + plan.dv
    vm = pltpu.VMEM
    n_mail = 5 * (plan.fs - 1) + 2 * ((1 << n_dims) - 1) * 2 + plan.tp
    scratch = [
        vm((width, made), BF16), vm((plan.dv, width), BF16), vm((width, ff), BF16), vm((width, ff), BF16),
        vm((ff, width), BF16),
        vm((shard, made), BF16), vm((plan.dv, shard), BF16), vm((shard, ff), BF16), vm((shard, ff), BF16),
        vm((ff, shard), BF16),
        vm((rows, width), BF16), vm((rows, width), BF16), vm((16, width), BF16),
        vm((length, DK // 2), F32), vm((length, DK // 2), F32), vm((PAD, ff), F32),
        vm((rows, 2 * plan.qk), BF16), vm((rows, plan.dv), BF16), vm((rows, plan.dv), BF16),
        vm((rows, width), BF16), vm((rows, ff), BF16), vm((ROWS + PAD, ff), F32),
    ]
    scratch += [vm((1 << (n_dims - 1 - k), length, block), BF16) for k in range(n_dims)]
    scratch += [vm((1 << (n_dims - 1 - k), length, block), BF16) for k in range(1, n_dims)]
    scratch += [
        pltpu.SemaphoreType.DMA((n_mail,)), pltpu.SemaphoreType.DMA((n_mail,)), pltpu.SemaphoreType.DMA((24,)),
    ]
    hbm = pl.BlockSpec(memory_space=pl.ANY)
    return pl.pallas_call(
        functools.partial(kernel, plan),
        out_shape=jax.ShapeDtypeStruct((length, block), BF16),
        in_specs=[hbm] * 7 + [pl.BlockSpec(memory_space=pltpu.SMEM)] + [hbm] * 5,
        out_specs=pl.BlockSpec(memory_space=pltpu.VMEM),
        scratch_shapes=scratch,
        compiler_params=pltpu.CompilerParams(
            collective_id=0, has_side_effects=True, vmem_limit_bytes=67043328
        ),
        name="layer",
    )(
        seq_rows, gains, cosine, sine, query_weight, key_weight, value_weight, decay_logs, mixer_out_weight,
        value_up_weight, gate_up_weight, conv, down_weight,
    )


def solution(mesh):
    placed = (
        P("fs", "tp"), P("tp"), P("fs", "tp"), P("fs", "tp"), P("fs", "tp"), P("tp"), P("tp", "fs"), P("tp"),
        P("fs", "tp"), P("fs", "tp"), P(None, "tp"), P("tp"), P("tp", "fs"),
    )
    return jax.shard_map(
        on_device, mesh=mesh, in_specs=placed, out_specs=P("fs", "tp"), check_vma=False
    )
```

profile of v0, /device:TPU:0, one launch (start us, length us, event | category | flops | bytes accessed | tf_op | source)
XLA Modules:
  0.0 291.6 jit_solution(15314484117188429147)
XLA Ops:
  0.0 0.1 pad.2.clone
  0.1 0.0 copy-start.2
  0.1 0.0 copy-start.3
  0.1 0.0 copy-start.1
  0.1 0.1 pad.5.clone
  0.2 0.6 copy-done.2
  0.8 0.0 copy-done.3
  0.8 0.0 copy-done.1
  0.8 0.0 copy-start
  0.8 0.7 maximum_maximum_fusion.gain_hbm
  1.5 0.0 copy-done
  1.5 0.7 maximum_convert_fusion.conv_hbm
  2.2 287.3 %layer.1 = bf16[768,512]{1,0:T(8,128)(2,1)} custom-call(bf16[768,512]{1,0:T(8,128)(2,1)} %x_hbm.1, bf16[16,512]{1,0:T(8,128)(2,1)} %maximum_maximum_fusion.gain_hbm, f32[768,128]{1,0:T(8,128)} %constant.2.clone.cos_hbm, f32[768,128]{1,0:T(8,128)} %constant.8.clone.sin_hbm, bf16[256,512]{1,0:T(8,128)(2,1)} %q_hbm.1, bf16[256,512]{1,0:T(8,128)(2,1)} %k_hbm.1, ...), custom_call_target="tpu_custom_call" | custom-call | tf_op jit(solution)/shard_map/layer/pallas_call | solution.py:499
  289.5 2.1 copy.17
  (5 shorter events, 0.0 us)
Async XLA Ops:
  0.1 0.7 copy-start.2
  0.1 0.7 copy-start.3
  0.1 0.7 copy-start.1
  0.8 0.7 copy-start
where the time goes:
time: 292 us
  Pallas kernels  287 us (98%)
    pallas_call x1, Pallas kernels, on_device(): pl.pallas_call(functools.partial(kernel, plan), out_shape=jax.ShapeDtypeS...  287 us

commit v1 on v0

v1 whole, which is shorter than its diff:
```python
import functools

import jax
import jax.numpy as jnp
import numpy as np
from jax import lax
from jax.experimental import pallas as pl
from jax.experimental.pallas import tpu as pltpu
from jax.sharding import PartitionSpec as P

DK = 256
DV = 512
KW = 3
EPS = 1e-06
ROPE_BASE = 10000.0
LANES = 128
ROWS = 256
PAD = 8
BF16 = jnp.bfloat16
F32 = jnp.float32


def flip(index, mask):
    return index + mask * (1 - 2 * lax.rem(lax.div(index, mask), 2))


def flips(index, mask):
    bit = 1
    while bit <= mask:
        if mask & bit:
            index = flip(index, bit)
        bit *= 2
    return index


def bits_of(size):
    return [1 << i for i in range(size.bit_length() - 1)]


class Plan:
    def __init__(self, fs, tp, length, block, heads_here, ff_here, shard):
        self.fs, self.tp, self.length, self.block, self.shard = fs, tp, length, block, shard
        self.width = fs * shard
        self.paired = heads_here % 2 == 0 and ff_here % LANES == 0 and fs >= 4
        self.heads = heads_here // 2 if self.paired else heads_here
        self.ff = -(-ff_here // (2 * LANES)) * LANES if self.paired else ff_here
        self.ff_step = ff_here - self.ff
        self.seqs = 2 if self.paired else 1
        self.rows = self.seqs * length
        self.pair = 2 if self.paired else 0
        bits = ([self.pair] if self.paired else []) + [b for b in bits_of(fs) if b > 1 and b != self.pair]
        self.near = 1
        self.far = []
        for bit in bits:
            self.far += [bit] + [c | bit for c in self.far]
        self.dims = [("tp", b) for b in bits_of(tp)] + ([("fs", self.pair)] if self.paired else [])
        self.qk = self.heads * DK
        self.dv = self.heads * DV
        self.heads_step = self.heads


class Mail:
    def __init__(self, sends, recvs, me):
        self.sends, self.recvs, self.me = sends, recvs, me
        self.count = 0
        self.ids = {}
        self.sent = []

    def id_of(self, key):
        if key not in self.ids:
            self.ids[key] = len(self.ids)
        return self.ids[key]

    def copy(self, key, src, dst, axis, mask):
        n = self.id_of(key)
        return pltpu.make_async_remote_copy(
            src_ref=src,
            dst_ref=dst,
            send_sem=self.sends.at[n],
            recv_sem=self.recvs.at[n],
            device_id={axis: flips(self.me[axis], mask)},
            device_id_type=pl.DeviceIdType.MESH,
        )

    def send(self, key, src, dst, axis, mask):
        copy = self.copy(key, src, dst, axis, mask)
        copy.start()
        self.sent.append((key, copy))
        return copy

    def arrive(self, key, slot, axis, mask):
        with jax.named_scope("wait_" + "_".join(str(k) for k in key)):
            self.copy(key, slot, slot, axis, mask).wait_recv()

    def drain(self, prefix):
        for key, copy in self.sent:
            if key[0].startswith(prefix):
                copy.wait_send()
        self.sent = [(key, copy) for key, copy in self.sent if not key[0].startswith(prefix)]


class Stream:
    def __init__(self, plan, mail, name, slot, stage):
        self.plan, self.mail, self.name, self.slot, self.stage = plan, mail, name, slot, stage
        self.mine = mail.me["fs"]
        self.far = list(plan.far)
        self.todo = [0] + list(plan.far)
        self.last = [c | plan.near for c in self.todo]
        self.turn = {True: 0, False: 0}

    def at(self, code):
        return self.slot(flips(self.mine, code))

    def send(self, times=1, who=None):
        for _ in range(times):
            for outer in (True, False) if who is None else (who == "outer",):
                self.turn[outer] += 1
            if who is None:
                if self.turn[True] <= len(self.far):
                    self.copy_of(self.far[self.turn[True] - 1]).start()
                continue
            turn = self.turn[who == "outer"]
            if turn > len(self.far):
                continue
            copy = self.copy_of(self.far[turn - 1])

            @pl.when(self.mail.outer if who == "outer" else jnp.logical_not(self.mail.outer))
            def _():
                copy.start()

    def copy_of(self, code):
        key = (self.name, code)
        src = self.stage if code & self.plan.pair else self.at(0)
        copy = self.mail.copy(key, src, self.at(0), "fs", code)
        if not any(k == key for k, _ in self.mail.sent):
            self.mail.sent.append((key, copy))
        return copy

    def cross(self, times=1):
        for _ in range(times):
            if self.todo:
                code = self.todo.pop(0)
                if code:
                    self.mail.arrive((self.name, code), self.at(code), "fs", code)
                self.mail.send((self.name, "x", code), self.at(code), self.at(code), "fs", self.plan.near)

    def finish(self):
        for who in ("outer", "inner"):
            self.send(max(0, len(self.far) - self.turn[who == "outer"]), who)
        self.cross(len(self.todo))
        for code in self.last:
            self.mail.arrive((self.name, "x", code & ~self.plan.near), self.at(code), "fs", self.plan.near)


def kernel(
    plan,
    x_hbm, gain_hbm, cos_hbm, sin_hbm, q_hbm, k_hbm, v_hbm, decay, out_hbm, val_hbm, gate_hbm, conv_hbm, down_hbm,
    result,
    w_in, w_out, w_val, w_gate, w_down, s_in, s_out, s_val, s_gate, s_down,
    act, act2, gains, cosine, sine, conv_par, qk, value, normed, part, hidden, gates, tail,
    *rest,
):
    n_dims = len(plan.dims)
    recvs, outs = rest[:n_dims], rest[n_dims : 2 * n_dims - 1]
    sends, arrivals, local = rest[2 * n_dims - 1 :]
    me = {"fs": lax.axis_index("fs"), "tp": lax.axis_index("tp")}
    length, block, shard = plan.length, plan.block, plan.shard
    row_blocks = length // ROWS
    seq = lax.rem(lax.div(me["fs"], plan.pair), 2) if plan.paired else 0

    barrier = pltpu.get_barrier_semaphore()
    near = [("fs", b) for b in plan.far + [plan.near]] + [d for d in plan.dims if d[0] == "tp"]
    for axis, bit in near:
        pl.semaphore_signal(
            barrier, inc=1, device_id={axis: flips(me[axis], bit)}, device_id_type=pl.DeviceIdType.MESH
        )

    places = []

    def fetch(src, dst):
        copy = pltpu.make_async_copy(src, dst, local.at[len(places)])
        copy.start()
        places.append(copy)

    def columns(index, width, size=None):
        return pl.ds(pl.multiple_of(index * width, width), size or width)

    def own_block(ref, s, t):
        return ref.at[columns(s, length), columns(t, block)]

    fetch(x_hbm, own_block(act, seq, me["tp"]))
    fetch(gain_hbm, gains.at[:, columns(me["tp"], block)])
    mine = me["fs"]
    rows_in = columns(mine, shard)

    def halves(dst, stage, take):
        fetch(take(seq), dst)
        if plan.paired:
            fetch(take(1 - seq), stage)

    qk_w, dv_w = plan.qk, plan.dv
    halves(w_in.at[rows_in, 0:qk_w], s_in.at[:, 0:qk_w], lambda h: q_hbm.at[:, columns(h, qk_w)])
    halves(
        w_in.at[rows_in, qk_w : 2 * qk_w], s_in.at[:, qk_w : 2 * qk_w], lambda h: k_hbm.at[:, columns(h, qk_w)]
    )
    halves(
        w_in.at[rows_in, 2 * qk_w : 2 * qk_w + dv_w],
        s_in.at[:, 2 * qk_w : 2 * qk_w + dv_w],
        lambda h: v_hbm.at[:, columns(h, dv_w)],
    )
    n_first = len(places)
    halves(w_out.at[:, columns(mine, shard)], s_out, lambda h: out_hbm.at[columns(h, dv_w), :])

    def ff_part(h):
        if not plan.paired:
            return slice(None)
        return pl.ds(pl.multiple_of(h * plan.ff_step, LANES), plan.ff)

    halves(w_val.at[rows_in, :], s_val, lambda h: val_hbm.at[:, ff_part(h)])
    halves(w_gate.at[rows_in, :], s_gate, lambda h: gate_hbm.at[:, ff_part(h)])
    halves(w_down.at[:, columns(mine, shard)], s_down, lambda h: down_hbm.at[ff_part(h), :])
    fetch(cos_hbm, cosine)
    fetch(sin_hbm, sine)
    fetch(conv_hbm.at[:, ff_part(seq)], conv_par)

    mail = Mail(sends, arrivals, me)
    top = plan.fs // 2
    mail.outer = lax.rem(lax.div(me["fs"], 2), 2) == lax.rem(lax.div(me["fs"], top), 2)
    st_in = Stream(plan, mail, "in", lambda j: w_in.at[columns(j, shard), :], s_in)
    st_out = Stream(plan, mail, "out", lambda j: w_out.at[:, columns(j, shard)], s_out)
    st_val = Stream(plan, mail, "val", lambda j: w_val.at[columns(j, shard), :], s_val)
    st_gate = Stream(plan, mail, "gate", lambda j: w_gate.at[columns(j, shard), :], s_gate)
    st_down = Stream(plan, mail, "down", lambda j: w_down.at[:, columns(j, shard)], s_down)

    def seq_of(dims, code):
        for place, (axis, _) in enumerate(dims):
            if axis == "fs" and code >> place & 1:
                return 1 - seq
        return seq

    def tp_of(dims, code):
        return flips(me["tp"], sum(bit for k, (axis, bit) in enumerate(dims) if axis == "tp" and code >> k & 1))

    def low(code):
        return next(i for i in range(n_dims) if code >> i & 1) if code else n_dims

    class Gather:
        def __init__(self, name, at, dims):
            self.name, self.at, self.dims = name, at, dims
            self.todo = []
            codes = [0]
            for place in range(len(self.dims) - 1, -1, -1):
                new = [c | (1 << place) for c in codes]
                self.todo += [(c, place) for c in new]
                codes = codes + new

        def forward(self, code, last):
            for place in range(last - 1, -1, -1):
                axis, bit = self.dims[place]
                mail.send((self.name, place, code), self.at(code), self.at(code), axis, bit)

        def begin(self):
            self.forward(0, len(self.dims))

        def step(self, times):
            for _ in range(times):
                if self.todo:
                    code, place = self.todo.pop(0)
                    axis, bit = self.dims[place]
                    mail.arrive((self.name, place, code & ~(1 << place)), self.at(code), axis, bit)
                    self.forward(code, place)

        def finish(self):
            self.step(len(self.todo))

    def block_rows(s, i):
        return pl.ds(pl.multiple_of(s * length + i * ROWS, ROWS), ROWS)

    class Scatter:
        def __init__(self, name, i, dims):
            self.name, self.i, self.dims = name, i, dims
            self.rows = slice(i * ROWS, (i + 1) * ROWS)
            self.waited = set()

        def multiply(self, left, right):
            def body(n, _):
                rows = block_rows(lax.div(n, plan.tp), self.i)
                cols = columns(lax.rem(n, plan.tp), block)
                part[rows, cols] = jnp.dot(left[rows, :], right[:, cols], preferred_element_type=F32).astype(BF16)
                return 0

            with jax.named_scope(f"multiply_{self.name}"):
                lax.fori_loop(0, plan.seqs * plan.tp, body, 0)
            for code in range((1 << n_dims) - 1, 0, -2):
                self.ship(code, part.at[self.term(code)])

        def term(self, code):
            return block_rows(seq_of(self.dims, code), self.i), columns(tp_of(self.dims, code), block)

        def slot(self, place, code):
            return recvs[place].at[code >> (place + 1), self.rows]

        def ship(self, code, src):
            place = low(code)
            axis, bit = self.dims[place]
            mail.send((self.name, place, code), src, self.slot(place, code), axis, bit)

        def summed(self, code):
            for k in range(low(code)):
                axis, bit = self.dims[k]
                mail.arrive((self.name, k, code | (1 << k)), self.slot(k, code), axis, bit)
            with jax.named_scope(f"sum_{self.name}_{code}"):
                total = part[self.term(code)].astype(F32)
                for k in range(low(code)):
                    total = total + recvs[k][code >> (k + 1), self.rows].astype(F32)
            return total

        def stage(self, place):
            for code in [c for c in range(1 << n_dims) if low(c) == place][::-1]:
                outs[place - 1][code >> (place + 1), self.rows] = self.summed(code).astype(BF16)
                self.ship(code, outs[place - 1].at[code >> (place + 1), self.rows])

    tp_dims = [d for d in plan.dims if d[0] == "tp"]
    gather_gain = Gather("gain", lambda c: gains.at[:, columns(tp_of(tp_dims, c), block)], tp_dims)
    gather_one = Gather(
        "one", lambda c: own_block(act, seq_of(plan.dims, c), tp_of(plan.dims, c)), plan.dims
    )

    def gather_two(i):
        def at(c):
            return act2.at[block_rows(seq_of(plan.dims, c), i), columns(tp_of(plan.dims, c), block)]

        return Gather(f"two{i}", at, plan.dims)

    for copy in places[:n_first]:
        copy.wait()
    with jax.named_scope("barrier"):
        pl.semaphore_wait(barrier, len(near))
    st_in.send(1)
    st_in.cross(1)
    gather_one.begin()
    st_in.send(2)
    gather_gain.begin()
    for copy in places[n_first:]:
        copy.wait()
    st_out.cross(1)
    st_val.cross(1)
    st_in.cross(2)
    gather_one.step(1)
    st_in.cross(1)
    st_out.send(3)
    gather_one.step(2)
    gather_gain.step(1)
    st_out.cross(1)
    st_val.send(3)
    st_out.cross(1)
    gather_one.finish()
    gather_gain.finish()
    st_in.finish()

    def scaled_rows(ref, start, gain_row):
        rows_f = ref[pl.ds(start, ROWS), :].astype(F32)
        factor = lax.rsqrt(jnp.mean(rows_f * rows_f, axis=-1, keepdims=True) + EPS)
        gain = gains[gain_row : gain_row + 1, :].astype(F32)
        return (rows_f * gain).astype(BF16), factor

    def project(i, _):
        start = pl.multiple_of(i * ROWS, ROWS)
        spot = pl.ds(pl.multiple_of(lax.rem(i, row_blocks) * ROWS, ROWS), ROWS)
        scaled, factor = scaled_rows(act, start, 0)
        total = jnp.dot(scaled, w_in[...], preferred_element_type=F32)
        cos, sin = cosine[spot, :], sine[spot, :]
        half = DK // 2
        for which, scale in ((0, 1.0), (1, DK**-0.5)):
            for head in range(plan.heads):
                at = which * qk_w + head * DK
                turned = (total[:, at : at + DK] * factor).astype(BF16).astype(F32)
                one, two = turned[:, :half], turned[:, half:]
                qk[pl.ds(start, ROWS), at : at + half] = ((one * cos - two * sin) * scale).astype(BF16)
                qk[pl.ds(start, ROWS), at + half : at + DK] = ((one * sin + two * cos) * scale).astype(BF16)
        value[pl.ds(start, ROWS), :] = (total[:, 2 * qk_w :] * factor).astype(BF16)
        return 0

    for s in range(plan.seqs):
        with jax.named_scope("project"):
            lax.fori_loop(s * row_blocks, (s + 1) * row_blocks, project, 0)
        st_out.cross(1)

    def retain(s, _):
        for head in range(plan.heads):
            log_decay = decay[seq * plan.heads + head]
            for b in range(row_blocks):
                seen = (b + 1) * ROWS
                first = pl.multiple_of(s * length, ROWS)
                rows = pl.ds(pl.multiple_of(first + b * ROWS, ROWS), ROWS)
                keys = pl.ds(first, seen)
                query = qk[rows, head * DK : (head + 1) * DK]
                key = qk[keys, qk_w + head * DK : qk_w + (head + 1) * DK]
                scores = lax.dot_general(query, key, (((1,), (1,)), ((), ())), preferred_element_type=F32)
                spread = (
                    lax.broadcasted_iota(jnp.int32, (ROWS, seen), 0)
                    - lax.broadcasted_iota(jnp.int32, (ROWS, seen), 1)
                    + b * ROWS
                )
                fall = jnp.exp(log_decay * jnp.maximum(spread, 0).astype(F32))
                scores = jnp.where(spread >= 0, scores * fall, 0.0).astype(BF16)
                ret = jnp.dot(scores, value[keys, head * DV : (head + 1) * DV], preferred_element_type=F32)
                centred = ret - jnp.mean(ret, axis=-1, keepdims=True)
                scale = lax.rsqrt(jnp.mean(centred * centred, axis=-1, keepdims=True) + EPS)
                normed[rows, head * DV : (head + 1) * DV] = (centred * scale).astype(BF16)
        return 0

    with jax.named_scope("retain"):
        lax.fori_loop(0, plan.seqs, retain, 0)
    st_gate.send(3, "inner")
    st_out.finish()

    chunks = range(row_blocks)
    own_cols = columns(me["tp"], block)
    first_sums = [Scatter(f"mixed{i}", i, plan.dims) for i in chunks]
    gathers = [gather_two(i) for i in chunks]

    def middle(i):
        mine_rows = block_rows(seq, i)
        act2[mine_rows, own_cols] = (act[mine_rows, own_cols].astype(F32) + first_sums[i].summed(0)).astype(BF16)
        gathers[i].begin()

    def stages(sums, which):
        for i in which:
            for place in range(2, n_dims):
                sums[i].stage(place)

    for i in chunks:
        first_sums[i].multiply(normed, w_out)
        first_sums[i].stage(1)
    st_val.cross(1)
    stages(first_sums, [0])
    stages(first_sums, [1])
    st_val.cross(1)
    stages(first_sums, list(chunks)[2:])
    st_gate.send(2, "outer")
    st_val.cross(1)
    middle(0)
    st_gate.cross(1)
    st_down.cross(1)
    middle(1)
    for i in chunks[2:]:
        middle(i)
    st_gate.send(1, "outer")
    st_down.send(3)
    gathers[0].step(1)
    st_gate.cross(1)
    for i in chunks[1:]:
        gathers[i].step(1)
    st_gate.cross(1)
    gathers[0].step(2)
    gathers[1].step(2)
    st_gate.cross(1)
    gathers[2].step(2)
    st_down.cross(1)
    st_val.finish()
    st_gate.finish()

    column = lax.broadcasted_iota(jnp.int32, (1, plan.ff), 1)
    keep = column >= seq * (plan.ff - plan.ff_step) if plan.paired else None

    def expand(i):
        def body(s, _):
            start = pl.multiple_of(s * length + i * ROWS, ROWS)
            scaled, factor = scaled_rows(act2, start, 1)
            gate = (jnp.dot(scaled, w_gate[...], preferred_element_type=F32) * factor).astype(BF16).astype(F32)
            if i:
                gates[0:PAD, :] = tail[s]
            else:
                gates[0:PAD, :] = jnp.zeros((PAD, plan.ff), F32)
            gates[PAD : PAD + ROWS, :] = gate
            tail[s] = gates[ROWS : ROWS + PAD, :]
            conv = conv_par[KW : KW + 1, :] + jnp.zeros((ROWS, plan.ff), F32)
            for tap in range(KW):
                at = PAD - KW + 1 + tap
                conv = conv + conv_par[tap : tap + 1, :] * gates[at : at + ROWS, :]
            up = (jnp.dot(scaled, w_val[...], preferred_element_type=F32) * factor).astype(BF16).astype(F32)
            made = conv / (1.0 + jnp.exp(-conv)) * up
            if keep is not None:
                made = jnp.where(keep, made, 0.0)
            hidden[pl.ds(start, ROWS), :] = made.astype(BF16)
            return 0

        with jax.named_scope("expand"):
            lax.fori_loop(0, plan.seqs, body, 0)

    for i in chunks:
        gathers[i].finish()
        expand(i)
        st_down.cross(1)
    st_down.finish()
    mail.drain("mixed")

    turned_dims = plan.dims[:1] + plan.dims[1:][::-1]
    last_sums = [Scatter(f"channel{i}", i, turned_dims if i % 2 else plan.dims) for i in chunks]

    def finish_rows(i):
        total = act2[block_rows(seq, i), own_cols].astype(F32) + last_sums[i].summed(0)
        result[last_sums[i].rows, :] = total.astype(BF16)

    for i in chunks:
        last_sums[i].multiply(hidden, w_down)
        last_sums[i].stage(1)
    for i in chunks:
        stages(last_sums, [i])
        if i:
            finish_rows(i - 1)
    finish_rows(row_blocks - 1)
    mail.drain("")


def on_device(
    seq_rows, mixer_gain, query_weight, key_weight, value_weight, decay_logs, mixer_out_weight, channel_gain,
    value_up_weight, gate_up_weight, conv_taps, conv_bias, down_weight,
):
    length, block = seq_rows.shape
    plan = Plan(
        lax.axis_size("fs"), lax.axis_size("tp"), length, block,
        query_weight.shape[1] // DK, value_up_weight.shape[1], query_weight.shape[0],
    )
    gains = jnp.concatenate(
        [mixer_gain[None], channel_gain[None], jnp.zeros((14, block), BF16)], axis=0
    )
    conv = jnp.concatenate(
        [conv_taps, conv_bias[None], jnp.zeros((PAD - KW - 1, conv_bias.shape[0]), BF16)], axis=0
    ).astype(F32)
    freqs = np.power(np.float32(ROPE_BASE), -np.arange(DK // 2, dtype=np.float32) * np.float32(2.0) / np.float32(DK))
    angles = np.arange(length, dtype=np.float32)[:, None] * freqs[None, :].astype(np.float32)
    cosine = jnp.asarray(np.cos(angles).astype(np.float32))
    sine = jnp.asarray(np.sin(angles).astype(np.float32))
    n_dims = len(plan.dims)
    rows, ff, width, shard = plan.rows, plan.ff, plan.width, plan.shard
    made = 2 * plan.qk + plan.dv
    vm = pltpu.VMEM
    n_mail = 5 * plan.fs + ((1 << n_dims) - 1) * (1 + 3 * (length // ROWS)) + plan.tp
    scratch = [
        vm((width, made), BF16), vm((plan.dv, width), BF16), vm((width, ff), BF16), vm((width, ff), BF16),
        vm((ff, width), BF16),
        vm((shard, made), BF16), vm((plan.dv, shard), BF16), vm((shard, ff), BF16), vm((shard, ff), BF16),
        vm((ff, shard), BF16),
        vm((rows, width), BF16), vm((rows, width), BF16), vm((16, width), BF16),
        vm((length, DK // 2), F32), vm((length, DK // 2), F32), vm((PAD, ff), F32),
        vm((rows, 2 * plan.qk), BF16), vm((rows, plan.dv), BF16), vm((rows, plan.dv), BF16),
        vm((rows, width), BF16), vm((rows, ff), BF16), vm((ROWS + PAD, ff), F32), vm((plan.seqs, PAD, ff), F32),
    ]
    scratch += [vm((1 << (n_dims - 1 - k), length, block), BF16) for k in range(n_dims)]
    scratch += [vm((1 << (n_dims - 1 - k), length, block), BF16) for k in range(1, n_dims)]
    scratch += [
        pltpu.SemaphoreType.DMA((n_mail,)), pltpu.SemaphoreType.DMA((n_mail,)), pltpu.SemaphoreType.DMA((24,)),
    ]
    hbm = pl.BlockSpec(memory_space=pl.ANY)
    return pl.pallas_call(
        functools.partial(kernel, plan),
        out_shape=jax.ShapeDtypeStruct((length, block), BF16),
        in_specs=[hbm] * 7 + [pl.BlockSpec(memory_space=pltpu.SMEM)] + [hbm] * 5,
        out_specs=pl.BlockSpec(memory_space=pltpu.VMEM),
        scratch_shapes=scratch,
        compiler_params=pltpu.CompilerParams(
            collective_id=0, has_side_effects=True, vmem_limit_bytes=67043328
        ),
        name="layer",
    )(
        seq_rows, gains, cosine, sine, query_weight, key_weight, value_weight, decay_logs, mixer_out_weight,
        value_up_weight, gate_up_weight, conv, down_weight,
    )


def solution(mesh):
    placed = (
        P("fs", "tp"), P("tp"), P("fs", "tp"), P("fs", "tp"), P("fs", "tp"), P("tp"), P("tp", "fs"), P("tp"),
        P("fs", "tp"), P("fs", "tp"), P(None, "tp"), P("tp"), P("tp", "fs"),
    )
    return jax.shard_map(
        on_device, mesh=mesh, in_specs=placed, out_specs=P("fs", "tp"), check_vma=False
    )
```

time: 292 us -> 251 us (0.86)
  Pallas kernels: 287 us -> 246 us
    pallas_call x1, Pallas kernels: 287 us -> 246 us  [on_device(): pl.pallas_call(functools.partial(kernel, plan), out_shape=jax.ShapeDtypeS...]
where the time goes in v1:
time: 251 us
  Pallas kernels  246 us (98%)
  local copies, waits for them, and re-layouts  2.89 us (1%)
    pallas_call x1, Pallas kernels, on_device(): pl.pallas_call(functools.partial(kernel, plan), out_shape=jax.ShapeDtypeS...  246 us

profile of v1, /device:TPU:0, one launch (start us, length us, event | category | flops | bytes accessed | tf_op | source)
XLA Modules:
  0.0 250.6 jit_solution(4996665858513479871)
XLA Ops:
  0.0 0.1 pad.2.clone
  0.1 0.0 copy-start.2
  0.1 0.0 copy-start.3
  0.1 0.0 copy-start.1
  0.1 0.1 pad.5.clone
  0.2 0.6 copy-done.2
  0.8 0.0 copy-done.3
  0.8 0.0 copy-done.1
  0.8 0.0 copy-start
  0.8 0.7 maximum_maximum_fusion.gain_hbm
  1.5 0.0 copy-done
  1.5 0.7 maximum_convert_fusion.conv_hbm
  2.2 246.3 %layer.1 = bf16[768,512]{1,0:T(8,128)(2,1)} custom-call(bf16[768,512]{1,0:T(8,128)(2,1)} %x_hbm.1, bf16[16,512]{1,0:T(8,128)(2,1)} %maximum_maximum_fusion.gain_hbm, f32[768,128]{1,0:T(8,128)} %constant.2.clone.cos_hbm, f32[768,128]{1,0:T(8,128)} %constant.8.clone.sin_hbm, bf16[256,512]{1,0:T(8,128)(2,1)} %q_hbm.1, bf16[256,512]{1,0:T(8,128)(2,1)} %k_hbm.1, ...), custom_call_target="tpu_custom_call" | custom-call | tf_op jit(solution)/shard_map/layer/pallas_call | solution.py:557
  248.6 2.1 copy.17
  (5 shorter events, 0.0 us)
Async XLA Ops:
  0.1 0.7 copy-start.2
  0.1 0.7 copy-start.3
  0.1 0.7 copy-start.1
  0.8 0.7 copy-start

commit v2 on v1

--- a/solution.py
+++ b/solution.py
@@ -16,6 +16,10 @@
 LANES = 128
 ROWS = 256
 PAD = 8
+LAST_CUTS = 4
+SCHEDULE = (
+    ("gi", 3), "gc", "dc", "of", "m0", "m1", "vc", "m2", "s0", "s1", "vc", "s2", ("go", 2), "vc", "d0", "gc", "d1", "d2", ("go", 1), ("do", 3), ("di", 3), "g0", "g1", "gc", "g2", "gc", "h0", "h1", "h2", "dc", "vf", "gf", "e0", "dc", "e1", "e2",
+)
 BF16 = jnp.bfloat16
 F32 = jnp.float32
 
@@ -43,8 +47,12 @@
         self.width = fs * shard
         self.paired = heads_here % 2 == 0 and ff_here % LANES == 0 and fs >= 4
         self.heads = heads_here // 2 if self.paired else heads_here
-        self.ff = -(-ff_here // (2 * LANES)) * LANES if self.paired else ff_here
-        self.ff_step = ff_here - self.ff
+        self.packed = self.paired and ff_here % (2 * LANES) > 0
+        units = ff_here // 2 if self.paired else ff_here
+        self.even = units // LANES * LANES if self.packed else units
+        self.units = units
+        self.ff = self.even + LANES if self.packed else units
+        self.half = units - self.even
         self.seqs = 2 if self.paired else 1
         self.rows = self.seqs * length
         self.pair = 2 if self.paired else 0
@@ -72,7 +80,12 @@
         return self.ids[key]
 
     def copy(self, key, src, dst, axis, mask):
-        n = self.id_of(key)
+        return self.copy_by(self.id_of(key), src, dst, axis, mask)
+
+    def either(self, of_outer, of_inner):
+        return of_outer + (1 - self.outer.astype(jnp.int32)) * (of_inner - of_outer)
+
+    def copy_by(self, n, src, dst, axis, mask):
         return pltpu.make_async_remote_copy(
             src_ref=src,
             dst_ref=dst,
@@ -100,16 +113,17 @@
 
 
 class Stream:
-    def __init__(self, plan, mail, name, slot, stage):
-        self.plan, self.mail, self.name, self.slot, self.stage = plan, mail, name, slot, stage
+    def __init__(self, plan, mail, name, parts, slot, stage):
+        self.plan, self.mail, self.name, self.slot, self.stage, self.parts = plan, mail, name, slot, stage, parts
         self.mine = mail.me["fs"]
         self.far = list(plan.far)
-        self.todo = [0] + list(plan.far)
-        self.last = [c | plan.near for c in self.todo]
+        self.order = [0] + list(plan.far)
+        self.order_inner = self.order[:1] + self.order[-1:] + self.order[1:-1] if plan.paired and name in ("gate", "down") else self.order
+        self.crossed = self.landed = 0
         self.turn = {True: 0, False: 0}
 
-    def at(self, code):
-        return self.slot(flips(self.mine, code))
+    def at(self, code, part):
+        return self.slot(flips(self.mine, code), part)
 
     def send(self, times=1, who=None):
         for _ in range(times):
@@ -117,39 +131,72 @@
                 self.turn[outer] += 1
             if who is None:
                 if self.turn[True] <= len(self.far):
-                    self.copy_of(self.far[self.turn[True] - 1]).start()
+                    for copy in self.copies_of(self.far[self.turn[True] - 1]):
+                        copy.start()
                 continue
             turn = self.turn[who == "outer"]
             if turn > len(self.far):
                 continue
-            copy = self.copy_of(self.far[turn - 1])
+            copies = self.copies_of(self.far[turn - 1])
 
             @pl.when(self.mail.outer if who == "outer" else jnp.logical_not(self.mail.outer))
             def _():
-                copy.start()
-
-    def copy_of(self, code):
-        key = (self.name, code)
-        src = self.stage if code & self.plan.pair else self.at(0)
-        copy = self.mail.copy(key, src, self.at(0), "fs", code)
-        if not any(k == key for k, _ in self.mail.sent):
-            self.mail.sent.append((key, copy))
-        return copy
+                for copy in copies:
+                    copy.start()
+
+    def copies_of(self, code):
+        copies = []
+        for part in range(self.parts):
+            key = (self.name, part, code)
+            src = self.stage(part) if code & self.plan.pair else self.at(0, part)
+            copy = self.mail.copy(key, src, self.at(0, part), "fs", code)
+            copies.append(copy)
+            if not any(k == key for k, _ in self.mail.sent):
+                self.mail.sent.append((key, copy))
+        return copies
+
+    def code_at(self, place):
+        return self.order[place], self.order_inner[place]
+
+    def owner(self, place):
+        return self.mail.either(*(flips(self.mine, code) for code in self.code_at(place)))
+
+    def id_at(self, place, part, near):
+        keys = [(self.name, part, "x", c) if near else (self.name, part, c) for c in self.code_at(place)]
+        return self.mail.either(*(self.mail.id_of(key) for key in keys))
 
     def cross(self, times=1):
+        near = self.plan.near
         for _ in range(times):
-            if self.todo:
-                code = self.todo.pop(0)
-                if code:
-                    self.mail.arrive((self.name, code), self.at(code), "fs", code)
-                self.mail.send((self.name, "x", code), self.at(code), self.at(code), "fs", self.plan.near)
+            if self.crossed == len(self.order):
+                return
+            place = self.crossed
+            self.crossed += 1
+            for part in range(self.parts):
+                block = self.slot(self.owner(place), part)
+                if place:
+                    with jax.named_scope(f"wait_{self.name}_{part}_{place}"):
+                        self.mail.copy_by(self.id_at(place, part, False), block, block, "fs", near).wait_recv()
+                self.mail.copy_by(self.id_at(place, part, True), block, block, "fs", near).start()
+                code = self.order[place]
+                key = (self.name, part, "x", code)
+                block = self.at(code, part)
+                self.mail.sent.append((key, self.mail.copy(key, block, block, "fs", near)))
+
+    def land(self, place):
+        near = self.plan.near
+        self.landed = place + 1
+        for part in range(self.parts):
+            block = self.slot(flips(self.owner(place), near), part)
+            with jax.named_scope(f"wait_{self.name}_{part}_x{place}"):
+                self.mail.copy_by(self.id_at(place, part, True), block, block, "fs", near).wait_recv()
 
     def finish(self):
         for who in ("outer", "inner"):
             self.send(max(0, len(self.far) - self.turn[who == "outer"]), who)
-        self.cross(len(self.todo))
-        for code in self.last:
-            self.mail.arrive((self.name, "x", code & ~self.plan.near), self.at(code), "fs", self.plan.near)
+        self.cross(len(self.order) - self.crossed)
+        for place in range(self.landed, len(self.order)):
+            self.land(place)
 
 
 def kernel(
@@ -157,7 +204,7 @@
     x_hbm, gain_hbm, cos_hbm, sin_hbm, q_hbm, k_hbm, v_hbm, decay, out_hbm, val_hbm, gate_hbm, conv_hbm, down_hbm,
     result,
     w_in, w_out, w_val, w_gate, w_down, s_in, s_out, s_val, s_gate, s_down,
-    act, act2, gains, cosine, sine, conv_par, qk, value, normed, part, hidden, gates, tail,
+    act, act2, gains, cosine, sine, conv_par, qk, value, normed, part, hidden, gates, tail, tiles,
     *rest,
 ):
     n_dims = len(plan.dims)
@@ -211,26 +258,76 @@
     n_first = len(places)
     halves(w_out.at[:, columns(mine, shard)], s_out, lambda h: out_hbm.at[columns(h, dv_w), :])
 
+    even, half = plan.even, plan.half
+
     def ff_part(h):
         if not plan.paired:
             return slice(None)
-        return pl.ds(pl.multiple_of(h * plan.ff_step, LANES), plan.ff)
+        return pl.ds(pl.multiple_of(h * (plan.units + half), LANES), even)
 
     halves(w_val.at[rows_in, :], s_val, lambda h: val_hbm.at[:, ff_part(h)])
-    halves(w_gate.at[rows_in, :], s_gate, lambda h: gate_hbm.at[:, ff_part(h)])
-    halves(w_down.at[:, columns(mine, shard)], s_down, lambda h: down_hbm.at[ff_part(h), :])
+    halves(w_gate.at[rows_in, 0:even], s_gate.at[:, 0:even], lambda h: gate_hbm.at[:, ff_part(h)])
+    own_down = columns(mine, shard)
+    halves(w_down.at[0:even, own_down], s_down.at[0:even, :], lambda h: down_hbm.at[ff_part(h), :])
+    fetch(conv_hbm.at[:, ff_part(seq)], conv_par.at[:, 0:even])
+    if plan.packed:
+        middle_tile = slice(even, even + LANES)
+        halves(
+            w_down.at[even : even + half, own_down],
+            s_down.at[even : even + half, :],
+            lambda h: down_hbm.at[pl.ds(pl.multiple_of(even + h * half, half), half), :],
+        )
+        fetch(conv_hbm.at[:, middle_tile], conv_par.at[:, middle_tile])
+        fetch(val_hbm.at[:, middle_tile], tiles.at[0])
+        fetch(gate_hbm.at[:, middle_tile], tiles.at[1])
     fetch(cos_hbm, cosine)
     fetch(sin_hbm, sine)
-    fetch(conv_hbm.at[:, ff_part(seq)], conv_par)
+
+    def swap(tile):
+        return pltpu.roll(tile, half, 1)
+
+    def pack():
+        lower = lax.broadcasted_iota(jnp.int32, (1, LANES), 1) < half
+        val, gate, conv = tiles[0].astype(F32), tiles[1].astype(F32), conv_par[:, middle_tile]
+        first = jnp.where(lower, val, swap(gate))
+        second = jnp.where(lower, swap(val), gate)
+        w_gate[rows_in, middle_tile] = jnp.where(seq == 0, first, second).astype(BF16)
+        s_gate[:, middle_tile] = jnp.where(seq == 0, second, first).astype(BF16)
+        conv_par[:, middle_tile] = jnp.where(seq == 0, conv, swap(conv))
+        w_down[even + half : even + LANES, :] = jnp.zeros((LANES - half, plan.width), BF16)
 
     mail = Mail(sends, arrivals, me)
     top = plan.fs // 2
     mail.outer = lax.rem(lax.div(me["fs"], 2), 2) == lax.rem(lax.div(me["fs"], top), 2)
-    st_in = Stream(plan, mail, "in", lambda j: w_in.at[columns(j, shard), :], s_in)
-    st_out = Stream(plan, mail, "out", lambda j: w_out.at[:, columns(j, shard)], s_out)
-    st_val = Stream(plan, mail, "val", lambda j: w_val.at[columns(j, shard), :], s_val)
-    st_gate = Stream(plan, mail, "gate", lambda j: w_gate.at[columns(j, shard), :], s_gate)
-    st_down = Stream(plan, mail, "down", lambda j: w_down.at[:, columns(j, shard)], s_down)
+    def cut(size, n, part):
+        return slice(part * size // n, (part + 1) * size // n)
+
+    def rows_of(ref, j, n, part):
+        size = shard // n
+        return ref.at[pl.ds(pl.multiple_of(j * shard + part * size, size), size), :]
+
+    def cols_of(ref, j, rows):
+        return ref.at[rows, columns(j, shard)]
+
+    edges = (0, 2 * qk_w, 2 * qk_w + dv_w)
+    st_in = Stream(
+        plan, mail, "in", 2,
+        lambda j, p: w_in.at[columns(j, shard), edges[p] : edges[p + 1]], lambda p: s_in.at[:, edges[p] : edges[p + 1]],
+    )
+    st_out = Stream(
+        plan, mail, "out", 2,
+        lambda j, p: cols_of(w_out, j, cut(dv_w, 2, p)), lambda p: s_out.at[cut(dv_w, 2, p), :],
+    )
+    st_val = Stream(
+        plan, mail, "val", 2, lambda j, p: rows_of(w_val, j, 2, p), lambda p: s_val.at[cut(shard, 2, p), :]
+    )
+    st_gate = Stream(
+        plan, mail, "gate", 2, lambda j, p: rows_of(w_gate, j, 2, p), lambda p: s_gate.at[cut(shard, 2, p), :]
+    )
+    st_down = Stream(
+        plan, mail, "down", 2,
+        lambda j, p: cols_of(w_down, j, cut(plan.units, 2, p)), lambda p: s_down.at[cut(plan.units, 2, p), :],
+    )
 
     def seq_of(dims, code):
         for place, (axis, _) in enumerate(dims):
@@ -273,29 +370,31 @@
         def finish(self):
             self.step(len(self.todo))
 
-    def block_rows(s, i):
-        return pl.ds(pl.multiple_of(s * length + i * ROWS, ROWS), ROWS)
+    def block_rows(s, i, size=ROWS):
+        return pl.ds(pl.multiple_of(s * length + i * size, size), size)
 
     class Scatter:
-        def __init__(self, name, i, dims):
-            self.name, self.i, self.dims = name, i, dims
-            self.rows = slice(i * ROWS, (i + 1) * ROWS)
-            self.waited = set()
+        def __init__(self, name, i, dims, size=ROWS):
+            self.name, self.i, self.dims, self.size = name, i, dims, size
+            self.rows = slice(i * size, (i + 1) * size)
 
         def multiply(self, left, right):
             def body(n, _):
-                rows = block_rows(lax.div(n, plan.tp), self.i)
+                rows = block_rows(lax.div(n, plan.tp), self.i, self.size)
                 cols = columns(lax.rem(n, plan.tp), block)
                 part[rows, cols] = jnp.dot(left[rows, :], right[:, cols], preferred_element_type=F32).astype(BF16)
                 return 0
 
             with jax.named_scope(f"multiply_{self.name}"):
                 lax.fori_loop(0, plan.seqs * plan.tp, body, 0)
+            self.ship_first()
+
+        def ship_first(self):
             for code in range((1 << n_dims) - 1, 0, -2):
                 self.ship(code, part.at[self.term(code)])
 
         def term(self, code):
-            return block_rows(seq_of(self.dims, code), self.i), columns(tp_of(self.dims, code), block)
+            return block_rows(seq_of(self.dims, code), self.i, self.size), columns(tp_of(self.dims, code), block)
 
         def slot(self, place, code):
             return recvs[place].at[code >> (place + 1), self.rows]
@@ -343,6 +442,8 @@
     gather_gain.begin()
     for copy in places[n_first:]:
         copy.wait()
+    if plan.packed:
+        pack()
     st_out.cross(1)
     st_val.cross(1)
     st_in.cross(2)
@@ -412,8 +513,6 @@
 
     with jax.named_scope("retain"):
         lax.fori_loop(0, plan.seqs, retain, 0)
-    st_gate.send(3, "inner")
-    st_out.finish()
 
     chunks = range(row_blocks)
     own_cols = columns(me["tp"], block)
@@ -430,87 +529,115 @@
             for place in range(2, n_dims):
                 sums[i].stage(place)
 
-    for i in chunks:
-        first_sums[i].multiply(normed, w_out)
-        first_sums[i].stage(1)
-    st_val.cross(1)
-    stages(first_sums, [0])
-    stages(first_sums, [1])
-    st_val.cross(1)
-    stages(first_sums, list(chunks)[2:])
-    st_gate.send(2, "outer")
-    st_val.cross(1)
-    middle(0)
-    st_gate.cross(1)
-    st_down.cross(1)
-    middle(1)
-    for i in chunks[2:]:
-        middle(i)
-    st_gate.send(1, "outer")
-    st_down.send(3)
-    gathers[0].step(1)
-    st_gate.cross(1)
-    for i in chunks[1:]:
-        gathers[i].step(1)
-    st_gate.cross(1)
-    gathers[0].step(2)
-    gathers[1].step(2)
-    st_gate.cross(1)
-    gathers[2].step(2)
-    st_down.cross(1)
-    st_val.finish()
-    st_gate.finish()
-
-    column = lax.broadcasted_iota(jnp.int32, (1, plan.ff), 1)
-    keep = column >= seq * (plan.ff - plan.ff_step) if plan.paired else None
-
     def expand(i):
         def body(s, _):
             start = pl.multiple_of(s * length + i * ROWS, ROWS)
             scaled, factor = scaled_rows(act2, start, 1)
-            gate = (jnp.dot(scaled, w_gate[...], preferred_element_type=F32) * factor).astype(BF16).astype(F32)
+            both = (jnp.dot(scaled, w_gate[...], preferred_element_type=F32) * factor).astype(BF16).astype(F32)
             if i:
                 gates[0:PAD, :] = tail[s]
             else:
                 gates[0:PAD, :] = jnp.zeros((PAD, plan.ff), F32)
-            gates[PAD : PAD + ROWS, :] = gate
+            gates[PAD : PAD + ROWS, 0:even] = both[:, 0:even]
+            if plan.packed:
+                gates[PAD : PAD + ROWS, middle_tile] = swap(both[:, middle_tile])
             tail[s] = gates[ROWS : ROWS + PAD, :]
             conv = conv_par[KW : KW + 1, :] + jnp.zeros((ROWS, plan.ff), F32)
             for tap in range(KW):
                 at = PAD - KW + 1 + tap
                 conv = conv + conv_par[tap : tap + 1, :] * gates[at : at + ROWS, :]
             up = (jnp.dot(scaled, w_val[...], preferred_element_type=F32) * factor).astype(BF16).astype(F32)
-            made = conv / (1.0 + jnp.exp(-conv)) * up
-            if keep is not None:
-                made = jnp.where(keep, made, 0.0)
-            hidden[pl.ds(start, ROWS), :] = made.astype(BF16)
+            opened = conv / (1.0 + jnp.exp(-conv))
+            hidden[pl.ds(start, ROWS), 0:even] = (opened[:, 0:even] * up).astype(BF16)
+            if plan.packed:
+                lower = lax.broadcasted_iota(jnp.int32, (1, LANES), 1) < half
+                made = jnp.where(lower, opened[:, middle_tile] * both[:, middle_tile], 0.0)
+                hidden[pl.ds(start, ROWS), middle_tile] = made.astype(BF16)
             return 0
 
         with jax.named_scope("expand"):
             lax.fori_loop(0, plan.seqs, body, 0)
 
-    for i in chunks:
+    def first_terms(i):
+        first_sums[i].multiply(normed, w_out)
+        first_sums[i].stage(1)
+
+    def last_gather(i):
         gathers[i].finish()
         expand(i)
-        st_down.cross(1)
+
+    chunk_steps = {
+        "m": first_terms,
+        "s": lambda i: stages(first_sums, [i]),
+        "d": middle,
+        "g": lambda i: gathers[i].step(1),
+        "h": lambda i: gathers[i].step(2),
+        "e": last_gather,
+    }
+    streams = {"o": st_out, "v": st_val, "g": st_gate, "d": st_down}
+    pending = {letter: list(chunks) for letter in chunk_steps}
+
+    def run(letter, i):
+        for before in chunk_steps:
+            upto = i if before == letter else i + 1
+            while pending[before] and pending[before][0] < upto:
+                chunk_steps[before](pending[before].pop(0))
+            if before == letter:
+                break
+        if i in pending[letter]:
+            pending[letter].remove(i)
+            chunk_steps[letter](i)
+
+    for step in SCHEDULE:
+        step, times = (step, 1) if isinstance(step, str) else step
+        if step[1].isdigit():
+            if int(step[1]) < row_blocks:
+                run(step[0], int(step[1]))
+        elif step[1] == "c":
+            streams[step[0]].cross(times)
+        elif step[1] == "f":
+            streams[step[0]].finish()
+        else:
+            streams[step[0]].send(times, "outer" if step[1] == "o" else "inner")
+    run("e", row_blocks - 1)
+    mail.drain("mixed")
+
+    turned_dims = plan.dims[:1] + plan.dims[1:][::-1]
+    cuts = LAST_CUTS if length % (LAST_CUTS * 16) == 0 else row_blocks
+    size = length // cuts
+    last_sums = [Scatter(f"channel{i}", i, turned_dims if i % 2 else plan.dims, size) for i in range(cuts)]
+
+    def reduce_columns(place, first, count, step):
+        cols = columns(lax.div(st_down.owner(place), 2), 2 * shard)
+
+        def body(n, _):
+            rows = pl.ds(pl.multiple_of(first + n * step, size), size)
+            part[rows, cols] = jnp.dot(hidden[rows, :], w_down[:, cols], preferred_element_type=F32).astype(BF16)
+            return 0
+
+        with jax.named_scope(f"reduce_{place}"):
+            lax.fori_loop(0, count, body, 0)
+
+    last = len(st_down.order) - 1
+    for place in range(last):
+        st_down.cross(max(0, place + 3 - st_down.crossed))
+        st_down.land(place)
+        reduce_columns(place, 0, plan.seqs * cuts, size)
     st_down.finish()
-    mail.drain("mixed")
-
-    turned_dims = plan.dims[:1] + plan.dims[1:][::-1]
-    last_sums = [Scatter(f"channel{i}", i, turned_dims if i % 2 else plan.dims) for i in chunks]
 
     def finish_rows(i):
-        total = act2[block_rows(seq, i), own_cols].astype(F32) + last_sums[i].summed(0)
+        total = act2[block_rows(seq, i, size), own_cols].astype(F32) + last_sums[i].summed(0)
         result[last_sums[i].rows, :] = total.astype(BF16)
 
-    for i in chunks:
-        last_sums[i].multiply(hidden, w_down)
+    for i in range(cuts):
+        reduce_columns(last, i * size, plan.seqs, length)
+        last_sums[i].ship_first()
         last_sums[i].stage(1)
-    for i in chunks:
-        stages(last_sums, [i])
-        if i:
-            finish_rows(i - 1)
-    finish_rows(row_blocks - 1)
+        if i >= 2:
+            stages(last_sums, [i - 2])
+    stages(last_sums, range(max(cuts - 2, 0), cuts))
+    for i in range(cuts):
+        finish_rows(i)
     mail.drain("")
 
 
@@ -537,21 +664,22 @@
     rows, ff, width, shard = plan.rows, plan.ff, plan.width, plan.shard
     made = 2 * plan.qk + plan.dv
     vm = pltpu.VMEM
-    n_mail = 5 * plan.fs + ((1 << n_dims) - 1) * (1 + 3 * (length // ROWS)) + plan.tp
+    n_mail = 10 * plan.fs + ((1 << n_dims) - 1) * (1 + 2 * (length // ROWS) + LAST_CUTS) + plan.tp
     scratch = [
-        vm((width, made), BF16), vm((plan.dv, width), BF16), vm((width, ff), BF16), vm((width, ff), BF16),
+        vm((width, made), BF16), vm((plan.dv, width), BF16), vm((width, plan.even), BF16), vm((width, ff), BF16),
         vm((ff, width), BF16),
-        vm((shard, made), BF16), vm((plan.dv, shard), BF16), vm((shard, ff), BF16), vm((shard, ff), BF16),
-        vm((ff, shard), BF16),
+        vm((shard, made), BF16), vm((plan.dv, shard), BF16), vm((shard, plan.even), BF16), vm((shard, ff), BF16),
+        vm((plan.units, shard), BF16),
         vm((rows, width), BF16), vm((rows, width), BF16), vm((16, width), BF16),
         vm((length, DK // 2), F32), vm((length, DK // 2), F32), vm((PAD, ff), F32),
         vm((rows, 2 * plan.qk), BF16), vm((rows, plan.dv), BF16), vm((rows, plan.dv), BF16),
         vm((rows, width), BF16), vm((rows, ff), BF16), vm((ROWS + PAD, ff), F32), vm((plan.seqs, PAD, ff), F32),
+        vm((2, shard, LANES), BF16),
     ]
     scratch += [vm((1 << (n_dims - 1 - k), length, block), BF16) for k in range(n_dims)]
     scratch += [vm((1 << (n_dims - 1 - k), length, block), BF16) for k in range(1, n_dims)]
     scratch += [
-        pltpu.SemaphoreType.DMA((n_mail,)), pltpu.SemaphoreType.DMA((n_mail,)), pltpu.SemaphoreType.DMA((24,)),
+        pltpu.SemaphoreType.DMA((n_mail,)), pltpu.SemaphoreType.DMA((n_mail,)), pltpu.SemaphoreType.DMA((32,)),
     ]
     hbm = pl.BlockSpec(memory_space=pl.ANY)
     return pl.pallas_call(

time: 251 us -> 238 us (0.948)
  Pallas kernels: 246 us -> 234 us
    pallas_call x1, Pallas kernels: 246 us -> 234 us  [on_device(): pl.pallas_call(functools.partial(kernel, plan), out_shape=jax.ShapeDtypeS...]
where the time goes in v2:
time: 238 us
  Pallas kernels  234 us (98%)
  local copies, waits for them, and re-layouts  2.89 us (1%)
    pallas_call x1, Pallas kernels, on_device(): pl.pallas_call(functools.partial(kernel, plan), out_shape=jax.ShapeDtypeS...  234 us

profile of v2, /device:TPU:0, one launch (start us, length us, event | category | flops | bytes accessed | tf_op | source)
XLA Modules:
  0.0 237.8 jit_solution(16321950278554132751)
XLA Ops:
  0.0 0.1 pad.2.clone
  0.1 0.0 copy-start.2
  0.1 0.0 copy-start.3
  0.1 0.0 copy-start.1
  0.1 0.1 pad.5.clone
  0.2 0.6 copy-done.2
  0.8 0.0 copy-done.3
  0.8 0.0 copy-done.1
  0.8 0.0 copy-start
  0.8 0.7 maximum_maximum_fusion.gain_hbm
  1.5 0.0 copy-done
  1.5 0.7 maximum_convert_fusion.conv_hbm
  2.2 233.5 %layer.1 = bf16[768,512]{1,0:T(8,128)(2,1)} custom-call(bf16[768,512]{1,0:T(8,128)(2,1)} %x_hbm.1, bf16[16,512]{1,0:T(8,128)(2,1)} %maximum_maximum_fusion.gain_hbm, f32[768,128]{1,0:T(8,128)} %constant.2.clone.cos_hbm, f32[768,128]{1,0:T(8,128)} %constant.8.clone.sin_hbm, bf16[256,512]{1,0:T(8,128)(2,1)} %q_hbm.1, bf16[256,512]{1,0:T(8,128)(2,1)} %k_hbm.1, ...), custom_call_target="tpu_custom_call" | custom-call | tf_op jit(solution)/shard_map/layer/pallas_call | solution.py:685
  235.8 2.1 copy.17
  (5 shorter events, 0.0 us)
Async XLA Ops:
  0.1 0.7 copy-start.2
  0.1 0.7 copy-start.3
  0.1 0.7 copy-start.1
  0.8 0.7 copy-start

commit v3 on v2

--- a/solution.py
+++ b/solution.py
@@ -18,7 +18,7 @@
 PAD = 8
 LAST_CUTS = 4
 SCHEDULE = (
-    ("gi", 3), "gc", "dc", "of", "m0", "m1", "vc", "m2", "s0", "s1", "vc", "s2", ("go", 2), "vc", "d0", "gc", "d1", "d2", ("go", 1), ("do", 3), ("di", 3), "g0", "g1", "gc", "g2", "gc", "h0", "h1", "h2", "dc", "vf", "gf", "e0", "dc", "e1", "e2",
+    ("gi", 3), "gc", "dc", "of", "m0", "m1", "vc", "m2", "s0", "s1", "vc", "s2", ("go", 1), "vc", "d0", "gc", "d1", "d2", ("go", 2), ("do", 3), ("di", 3), "g0", "g1", "gc", "g2", "gc", "h0", "h1", "h2", "dc", "vf", "gf", "e0", "dc", "e1", "e2",
 )
 BF16 = jnp.bfloat16
 F32 = jnp.float32
@@ -632,10 +632,11 @@
     for i in range(cuts):
         reduce_columns(last, i * size, plan.seqs, length)
         last_sums[i].ship_first()
-        last_sums[i].stage(1)
-        if i >= 2:
-            stages(last_sums, [i - 2])
-    stages(last_sums, range(max(cuts - 2, 0), cuts))
+        if i % 2 or i == cuts - 1:
+            for k in range(i - i % 2, i + 1):
+                last_sums[k].stage(1)
+    for i in range(cuts):
+        stages(last_sums, [i])
     for i in range(cuts):
         finish_rows(i)
     mail.drain("")

time: 238 us -> 237 us (level)
  no operation moved by 1% of the time
where the time goes in v3:
time: 237 us
  Pallas kernels  232 us (98%)
  local copies, waits for them, and re-layouts  2.89 us (1%)
    pallas_call x1, Pallas kernels, on_device(): pl.pallas_call(functools.partial(kernel, plan), out_shape=jax.ShapeDtypeS...  232 us

profile of v3, /device:TPU:0, one launch (start us, length us, event | category | flops | bytes accessed | tf_op | source)
XLA Modules:
  0.0 236.6 jit_solution(8164636318802226354)
XLA Ops:
  0.0 0.1 pad.2.clone
  0.1 0.0 copy-start.2
  0.1 0.0 copy-start.3
  0.1 0.0 copy-start.1
  0.1 0.1 pad.5.clone
  0.2 0.6 copy-done.2
  0.8 0.0 copy-done.3
  0.8 0.0 copy-done.1
  0.8 0.0 copy-start
  0.8 0.7 maximum_maximum_fusion.gain_hbm
  1.5 0.0 copy-done
  1.5 0.7 maximum_convert_fusion.conv_hbm
  2.2 232.3 %layer.1 = bf16[768,512]{1,0:T(8,128)(2,1)} custom-call(bf16[768,512]{1,0:T(8,128)(2,1)} %x_hbm.1, bf16[16,512]{1,0:T(8,128)(2,1)} %maximum_maximum_fusion.gain_hbm, f32[768,128]{1,0:T(8,128)} %constant.2.clone.cos_hbm, f32[768,128]{1,0:T(8,128)} %constant.8.clone.sin_hbm, bf16[256,512]{1,0:T(8,128)(2,1)} %q_hbm.1, bf16[256,512]{1,0:T(8,128)(2,1)} %k_hbm.1, ...), custom_call_target="tpu_custom_call" | custom-call | tf_op jit(solution)/shard_map/layer/pallas_call | solution.py:686
  234.5 2.1 copy.17
  (5 shorter events, 0.0 us)
Async XLA Ops:
  0.1 0.7 copy-start.2
  0.1 0.7 copy-start.3
  0.1 0.7 copy-start.1
  0.8 0.7 copy-start

commit v4 on v3

--- a/solution.py
+++ b/solution.py
@@ -18,7 +18,7 @@
 PAD = 8
 LAST_CUTS = 4
 SCHEDULE = (
-    ("gi", 3), "gc", "dc", "of", "m0", "m1", "vc", "m2", "s0", "s1", "vc", "s2", ("go", 1), "vc", "d0", "gc", "d1", "d2", ("go", 2), ("do", 3), ("di", 3), "g0", "g1", "gc", "g2", "gc", "h0", "h1", "h2", "dc", "vf", "gf", "e0", "dc", "e1", "e2",
+    ("gi", 3), "gc", "dc", "of", "m0", "m1", "vc", "m2", "s0", "s1", "vc", "s2", ("go", 1), "d0", "vc", "gc", "d1", "d2", ("go", 2), ("di", 3), ("do", 3), "g0", "g1", "gc", "g2", "gc", "h0", "h1", "h2", "dc", "vf", "gf", "e0", "dc", "e1", "e2",
 )
 BF16 = jnp.bfloat16
 F32 = jnp.float32

time: 237 us -> 237 us (level)
  no operation moved by 1% of the time
where the time goes in v4:
time: 237 us
  Pallas kernels  232 us (98%)
  local copies, waits for them, and re-layouts  2.89 us (1%)
    pallas_call x1, Pallas kernels, on_device(): pl.pallas_call(functools.partial(kernel, plan), out_shape=jax.ShapeDtypeS...  232 us

profile of v4, /device:TPU:0, one launch (start us, length us, event | category | flops | bytes accessed | tf_op | source)
XLA Modules:
  0.0 236.6 jit_solution(9363286859046930443)
XLA Ops:
  0.0 0.1 pad.2.clone
  0.1 0.0 copy-start.2
  0.1 0.0 copy-start.3
  0.1 0.0 copy-start.1
  0.1 0.1 pad.5.clone
  0.2 0.6 copy-done.2
  0.8 0.0 copy-done.3
  0.8 0.0 copy-done.1
  0.8 0.0 copy-start
  0.8 0.7 maximum_maximum_fusion.gain_hbm
  1.5 0.0 copy-done
  1.5 0.7 maximum_convert_fusion.conv_hbm
  2.2 232.3 %layer.1 = bf16[768,512]{1,0:T(8,128)(2,1)} custom-call(bf16[768,512]{1,0:T(8,128)(2,1)} %x_hbm.1, bf16[16,512]{1,0:T(8,128)(2,1)} %maximum_maximum_fusion.gain_hbm, f32[768,128]{1,0:T(8,128)} %constant.2.clone.cos_hbm, f32[768,128]{1,0:T(8,128)} %constant.8.clone.sin_hbm, bf16[256,512]{1,0:T(8,128)(2,1)} %q_hbm.1, bf16[256,512]{1,0:T(8,128)(2,1)} %k_hbm.1, ...), custom_call_target="tpu_custom_call" | custom-call | tf_op jit(solution)/shard_map/layer/pallas_call | solution.py:686
  234.5 2.1 copy.17
  (5 shorter events, 0.0 us)
Async XLA Ops:
  0.1 0.7 copy-start.2
  0.1 0.7 copy-start.3
  0.1 0.7 copy-start.1
  0.8 0.7 copy-start
